TPU v7x, 32 devices: a whole 2x2x4 slice. The times are simulated.
32 devices in a mesh: grp: 2 (over y), fs: 4 (over z), tp: 4 (over x, core).
Axes of the slice: x: 2, y: 2, z: 4, core: 2. Of those that a mesh axis runs over, the one named last changes fastest.
Arguments:
- tokens: bfloat16 [512, 2048], P(('grp', 'fs')), parts along dimension 0, may hold values from -6 to 6
- routes: int32 [512, 2], P(('grp', 'fs')), parts along dimension 0, may hold values from 0 to 3, as said below
- route_logits: float32 [512, 2], P(('grp', 'fs')), parts along dimension 0, may hold values from -8 to 8
- gain: float32 [2048], P('fs'), may hold values from 0.1 to 1.9
- w_gate: float32 [4, 2048, 7168], P(None, 'fs', 'tp'), may hold values from -0.125 to 0.125
- w_up: float32 [4, 2048, 7168], P(None, 'fs', 'tp'), may hold values from -0.125 to 0.125
- w_down: float32 [4, 7168, 2048], P(None, 'fs', 'tp'), may hold values from -0.0625 to 0.0625
Outputs:
- gate_served: bfloat16 [8, 2048, 7168], P(('grp', 'tp'), None, 'fs'), parts along dimension 0
- up_served: bfloat16 [8, 2048, 7168], P(('grp', 'tp'), None, 'fs'), parts along dimension 0
- down_served: bfloat16 [8, 7168, 2048], P(('grp', 'tp'), 'fs'), parts along dimension 0
- mixed: bfloat16 [512, 2048], P(('grp', 'fs'), 'tp'), parts along dimension 0
There are 2 independent parts, one for each index of `grp`. A program takes and returns all parts, laid end to end along the dimension named above; an argument that names none is the same for every part. Nothing has to cross between parts.
Inputs may be any that keep to these rules, and one draw needn't show every extreme that they name: `routes`: each row names 2 different experts; every expert is named by some row.
All inputs are finite; a program needn't handle non-finite values.
Results may differ from a plain program's by a relative error of at most 0.0085.
Values may be sent and summed in bfloat16 or wider, within the bound.
A program may use at most 192 MiB of HBM per device.

v0:
```python
import jax
import jax.numpy as jnp
from jax import lax
from jax.sharding import PartitionSpec as P


def body(tokens, routes, route_logits, gain, w_gate, w_up, w_down):
    gate_cast = (w_gate * gain[None, :, None]).astype(jnp.bfloat16)
    up_cast = (w_up * gain[None, :, None]).astype(jnp.bfloat16)
    down_cast = w_down.astype(jnp.bfloat16)
    gate_tp, up_tp, down_served = (
        lax.all_to_all(gate_cast, "tp", split_axis=0, concat_axis=2, tiled=True),
        lax.all_to_all(up_cast, "tp", split_axis=0, concat_axis=2, tiled=True),
        lax.all_to_all(down_cast, "tp", split_axis=0, concat_axis=2, tiled=True),
    )
    gate_served, up_served = (
        lax.all_to_all(gate_tp, "fs", split_axis=2, concat_axis=1, tiled=True),
        lax.all_to_all(up_tp, "fs", split_axis=2, concat_axis=1, tiled=True),
    )
    values = tokens.astype(jnp.float32)
    mean_square = jnp.mean(values * values, axis=-1, keepdims=True)
    normed = (values * lax.rsqrt(mean_square + 1e-06)).astype(jnp.bfloat16)
    expert_id = lax.axis_index("tp")
    first = jax.nn.sigmoid(route_logits[:, 0] - route_logits[:, 1])
    second = jax.nn.sigmoid(route_logits[:, 1] - route_logits[:, 0])
    weight_col = first * (routes[:, 0] == expert_id).astype(jnp.float32)
    weight_col = (weight_col + second * (routes[:, 1] == expert_id).astype(jnp.float32)).astype(
        jnp.bfloat16
    )
    gate_local = gate_served[0]
    up_local = up_served[0]
    piece_rows = lax.all_gather(normed, "fs", axis=0, tiled=True)
    piece_weight = lax.all_gather(weight_col, "fs", axis=0, tiled=True)
    gate_act = jnp.dot(piece_rows, gate_local, preferred_element_type=jnp.float32)
    up_act = jnp.dot(piece_rows, up_local, preferred_element_type=jnp.float32)
    hidden_rows = jax.nn.silu(gate_act) * up_act * piece_weight[:, None].astype(jnp.float32)
    hidden = hidden_rows.astype(jnp.bfloat16)
    down_local = down_served[0]
    term = jnp.dot(hidden, down_local, preferred_element_type=jnp.float32)
    by_feature = lax.psum_scatter(term, "tp", scatter_dimension=1, tiled=True)
    mixed = lax.psum_scatter(by_feature, "fs", scatter_dimension=0, tiled=True)
    return (gate_served, up_served, down_served, mixed.astype(jnp.bfloat16))


def solution(mesh):
    return jax.shard_map(
        body,
        mesh=mesh,
        in_specs=(
            P(("grp", "fs"), None),
            P(("grp", "fs"), None),
            P(("grp", "fs"), None),
            P("fs"),
            P(None, "fs", "tp"),
            P(None, "fs", "tp"),
            P(None, "fs", "tp"),
        ),
        out_specs=(
            P(("grp", "tp"), None, "fs"),
            P(("grp", "tp"), None, "fs"),
            P(("grp", "tp"), "fs", None),
            P(("grp", "fs"), "tp"),
        ),
        check_vma=False,
    )
```

profile of v0, /device:TPU:0, one launch (start us, length us, event | category | flops | bytes accessed | tf_op | source)
XLA Modules:
  0.0 715.9 jit_solution(18152583940366378702)
XLA Ops:
  7.2 14.4 %copy.24 = f32[4,512,1792]{1,2,0:T(8,128)} copy(f32[4,512,1792]{2,1,0:T(8,128)} %param.11) | data formatting | bytes 29360128 | tf_op args[4]
  21.5 14.3 %copy.27 = f32[4,512,1792]{1,2,0:T(8,128)} copy(f32[4,512,1792]{2,1,0:T(8,128)} %param.12) | data formatting | bytes 29360128 | tf_op args[5]
  35.8 13.5 %multiply_convert_fusion = (bf16[4,512,1792]{1,2,0:T(8,128)(2,1)}, bf16[4,512,1792]{1,2,0:T(8,128)(2,1)S(1)}) fusion(f32[4,512,1792]{1,2,0:T(8,128)} %copy.27, f32[512]{0:T(512)S(1)} %copy-done.1, f32[4,512,1792]{1,2,0:T(8,128)} %copy.24), kind=kLoop, calls=%fused_computation | loop fusion | flops 14680064 | bytes 44042240 | tf_op jit(solution)/shard_map/convert_element_type | solution.py:9
  49.3 86.2 %all_to_all.90 = bf16[4,512,1792]{1,2,0:T(8,128)(2,1)} all-to-all(bf16[4,512,1792]{1,2,0:T(8,128)(2,1)S(1)} %get-tuple-element.17), channel_id=1, replica_groups=mesh['grp'=2,'fs'=4,'tp'=4] {'tp'}, dimensions={0} | all-to-all | bytes 14680064 | tf_op jit(solution)/shard_map/all_to_all | solution.py:12
  135.5 5.4 all-to-all-start.2
  140.9 13.7 %copy.39 = bf16[1,512,7168]{1,0,2:T(2,128)(2,1)} copy(bf16[1,512,7168]{1,2,0:T(8,128)(2,1)} %bitcast.47) | data formatting | bytes 14680064 | tf_op jit(solution)/shard_map/all_to_all | solution.py:12
  155.2 48.2 %reduce = bf16[7168,512]{1,0:T(8,128)(2,1)} reduce(bf16[7168,1,512]{2,1,0:T(2,128)(2,1)} %bitcast.43, bf16[]{:T(256)} %broadcast.43), dimensions={1}, to_apply=%bitcast.42.reduce_sub_computation | reduce | bytes 14680066
  203.4 9.0 %reshape.55 = bf16[4,2,458752]{2,1,0:T(2,128)(2,1)} reshape(bf16[7168,512]{1,0:T(8,128)(2,1)} %reduce) | data formatting | bytes 14680064
  212.4 10.5 %all-to-all-done.2 = bf16[4,512,1792]{1,2,0:T(8,128)(2,1)} async-done(((bf16[4,512,1792]{1,2,0:T(8,128)(2,1)}), bf16[4,512,1792]{1,2,0:T(8,128)(2,1)}, u32[]{:S(2)}, u32[]{:S(2)}) %all-to-all-start.2) | async-done | bytes 7340064 | tf_op jit(solution)/shard_map/all_to_all | solution.py:13
  222.8 5.7 all-to-all-start.1
  228.5 13.7 %copy.38 = bf16[1,512,7168]{1,0,2:T(2,128)(2,1)} copy(bf16[1,512,7168]{1,2,0:T(8,128)(2,1)} %bitcast.7) | data formatting | bytes 14680064 | tf_op jit(solution)/shard_map/all_to_all | solution.py:13
  242.2 48.2 %reduce.1 = bf16[7168,512]{1,0:T(8,128)(2,1)} reduce(bf16[7168,1,512]{2,1,0:T(2,128)(2,1)} %bitcast.44, bf16[]{:T(256)} %broadcast.43), dimensions={1}, to_apply=%bitcast.41.reduce_sub_computation | reduce | bytes 14680066
  290.4 9.0 %reshape.57 = bf16[4,2,458752]{2,1,0:T(2,128)(2,1)} reshape(bf16[7168,512]{1,0:T(8,128)(2,1)} %reduce.1) | data formatting | bytes 14680064
  299.4 90.4 %all-to-all-done.1 = bf16[4,2,458752]{2,1,0:T(2,128)(2,1)} async-done(((bf16[4,2,458752]{2,1,0:T(2,128)(2,1)}), bf16[4,2,458752]{2,1,0:T(2,128)(2,1)}, u32[]{:S(2)}, u32[]{:S(2)}) %all-to-all-start.1) | async-done | bytes 7340064 | tf_op jit(solution)/shard_map/all_to_all | solution.py:17
  389.8 5.5 all-to-all-start.3
  395.3 11.6 %copy.30 = bf16[4,1792,512]{1,2,0:T(8,128)(2,1)} copy(f32[4,1792,512]{2,1,0:T(8,128)} %param.13) | data formatting | bytes 22020096 | tf_op args[6]
  407.0 148.5 %all-to-all-done.3 = bf16[4,2,458752]{2,1,0:T(2,128)(2,1)} async-done(((bf16[4,2,458752]{2,1,0:T(2,128)(2,1)}), bf16[4,2,458752]{2,1,0:T(2,128)(2,1)}, u32[]{:S(2)}, u32[]{:S(2)}) %all-to-all-start.3) | async-done | bytes 7340064 | tf_op jit(solution)/shard_map/all_to_all | solution.py:18
  555.4 5.4 all-to-all-start.4
  561.1 0.8 fusion.4
  563.5 10.1 %all-reduce = bf16[256]{0:T(256)(128)(2,1)S(1)} all-reduce(bf16[256]{0:T(256)(128)(2,1)S(1)} %dynamic-update-slice), channel_id=2, replica_groups=mesh['grp'=2,'fs'=4,'tp'=4] {'fs'}, use_global_device_ids=true, to_apply=%add | all-reduce | flops 256 | bytes 1024
  573.7 11.3 %reshape.56 = bf16[7168,1,512]{2,1,0:T(2,128)(2,1)} reshape(bf16[4,2,458752]{2,1,0:T(2,128)(2,1)} %all-to-all-done.1) | data formatting | bytes 14680064
  585.0 10.4 %copy.34 = bf16[1,512,7168]{1,2,0:T(8,128)(2,1)} copy(bf16[1,512,7168]{1,0,2:T(2,128)(2,1)} %bitcast.45) | data formatting | bytes 14680064
  595.4 9.9 %copy.26 = bf16[1,4,512,1792]{3,2,1,0:T(8,128)(2,1)} copy(bf16[1,4,512,1792]{2,3,1,0:T(8,128)(2,1)} %bitcast.48) | data formatting | bytes 14680064 | tf_op jit(solution)/shard_map/all_to_all | solution.py:17
  605.3 11.3 %reshape.58 = bf16[7168,1,512]{2,1,0:T(2,128)(2,1)} reshape(bf16[4,2,458752]{2,1,0:T(2,128)(2,1)} %all-to-all-done.3) | data formatting | bytes 14680064
  616.6 10.4 %copy.35 = bf16[1,512,7168]{1,2,0:T(8,128)(2,1)} copy(bf16[1,512,7168]{1,0,2:T(2,128)(2,1)} %bitcast.46) | data formatting | bytes 14680064
  627.0 9.9 %copy.29 = bf16[1,4,512,1792]{3,2,1,0:T(8,128)(2,1)} copy(bf16[1,4,512,1792]{2,3,1,0:T(8,128)(2,1)} %bitcast.49) | data formatting | bytes 14680064 | tf_op jit(solution)/shard_map/all_to_all | solution.py:18
  637.0 5.5 fusion.7
  642.8 11.1 %fusion.2 = f32[256,2048]{1,0:T(8,128)} fusion(bf16[1792,2048]{0,1:T(8,128)(2,1)} %bitcast.18, bf16[256,2048]{1,0:T(8,128)(2,1)S(1)} %copy-done.4, bf16[2048,1792]{1,0:T(8,128)(2,1)} %bitcast.52, f32[256,1792]{1,0:T(8,128)S(1)} %fusion.7, f32[256]{0:T(256)S(1)} %convert_element_type.41), kind=kOutput, calls=%fused_computation.5 | convolution fusion | flops 3761307648 | bytes 19661824 | tf_op jit(solution)/shard_map/dot_general | solution.py:39
  653.9 29.7 %reduce-scatter.3.cloned.1.call-done = f32[256,512]{1,0:T(8,128)} async-done(((f32[256,2048]{1,0:T(8,128)}), f32[256,512]{1,0:T(8,128)}) %reduce-scatter.3.cloned.1.call-update) | async-done | bytes 524304 | tf_op jit(solution)/shard_map/reduce_scatter | solution.py:40
  683.7 10.4 %copy.33 = bf16[1,1792,2048]{2,1,0:T(8,128)(2,1)} copy(bf16[1,1792,2048]{1,2,0:T(8,128)(2,1)} %bitcast.12) | data formatting | bytes 14680064
  694.1 13.7 %reduce-scatter.5.cloned.1.call-done = f32[64,512]{1,0:T(8,128)} async-done(((f32[256,512]{1,0:T(8,128)}), f32[64,512]{1,0:T(8,128)}) %reduce-scatter.5.cloned.1.call-update) | async-done | bytes 131088 | tf_op jit(solution)/shard_map/reduce_scatter | solution.py:41
  707.8 1.5 convert_element_type.38
  (28 shorter events, 2.0 us)
Async XLA Ops:
  21.5 14.3 %copy-start.1 = (f32[512]{0:T(512)S(1)}, f32[512]{0:T(512)}, u32[]{:S(2)}) copy-start(f32[512]{0:T(512)} %param.10) | copy-start | bytes 6148
  135.5 87.3 %all-to-all-start.2 = ((bf16[4,512,1792]{1,2,0:T(8,128)(2,1)}), bf16[4,512,1792]{1,2,0:T(8,128)(2,1)}, u32[]{:S(2)}, u32[]{:S(2)}) async-start(bf16[4,512,1792]{1,2,0:T(8,128)(2,1)} %get-tuple-element.16), calls=%async_computation.2 | async-start | bytes 14680064 | tf_op jit(solution)/shard_map/all_to_all | solution.py:13
  222.8 167.0 %all-to-all-start.1 = ((bf16[4,2,458752]{2,1,0:T(2,128)(2,1)}), bf16[4,2,458752]{2,1,0:T(2,128)(2,1)}, u32[]{:S(2)}, u32[]{:S(2)}) async-start(bf16[4,2,458752]{2,1,0:T(2,128)(2,1)} %reshape.55), calls=%async_computation.1 | async-start | bytes 14680064 | tf_op jit(solution)/shard_map/all_to_all | solution.py:17
  389.8 165.6 %all-to-all-start.3 = ((bf16[4,2,458752]{2,1,0:T(2,128)(2,1)}), bf16[4,2,458752]{2,1,0:T(2,128)(2,1)}, u32[]{:S(2)}, u32[]{:S(2)}) async-start(bf16[4,2,458752]{2,1,0:T(2,128)(2,1)} %reshape.57), calls=%async_computation.3 | async-start | bytes 14680064 | tf_op jit(solution)/shard_map/all_to_all | solution.py:18
  407.0 154.0 %copy-start = (bf16[64,2048]{1,0:T(8,128)(2,1)S(1)}, bf16[64,2048]{1,0:T(8,128)(2,1)}, u32[]{:S(2)}) copy-start(bf16[64,2048]{1,0:T(8,128)(2,1)} %param.7) | copy-start | bytes 786436
  407.0 155.0 %copy-start.5 = (u32[32]{0:T(128)S(1)}, u32[32]{0:T(128)}, u32[]{:S(2)}) copy-start(u32[32]{0:T(128)} %constant.19) | copy-start | bytes 388
  407.0 156.3 %copy-start.2 = (s32[64,2]{0,1:T(2,128)S(1)}, s32[64,2]{0,1:T(2,128)}, u32[]{:S(2)}) copy-start(s32[64,2]{0,1:T(2,128)} %param.8) | copy-start | bytes 1540
  407.0 156.3 %copy-start.3 = (f32[64,2]{0,1:T(2,128)S(1)}, f32[64,2]{0,1:T(2,128)}, u32[]{:S(2)}) copy-start(f32[64,2]{0,1:T(2,128)} %param.9) | copy-start | bytes 1540
  555.4 87.3 %all-to-all-start.4 = ((bf16[4,1792,512]{1,2,0:T(8,128)(2,1)}), bf16[4,1792,512]{1,2,0:T(8,128)(2,1)}, u32[]{:S(2)}, u32[]{:S(2)}) async-start(bf16[4,1792,512]{1,2,0:T(8,128)(2,1)} %copy.30), calls=%async_computation.4 | async-start | bytes 14680064 | tf_op jit(solution)/shard_map/all_to_all | solution.py:14
  560.9 76.1 %all-gather.3.cloned.1.call-start = ((), (), s32[]{:S(2)}) async-start(), calls=%async_computation.7 | async-start | bytes 1310720 | tf_op jit(solution)/shard_map/all_gather | solution.py:32
  561.9 121.7 %reduce-scatter.3.cloned.1.call-start = ((), (), s32[]{:S(2)}) async-start(), calls=%async_computation.8 | async-start | bytes 2621440 | tf_op jit(solution)/shard_map/reduce_scatter | solution.py:40
  637.0 5.8 copy-start.4
  653.9 53.9 %reduce-scatter.5.cloned.1.call-start = ((), (), s32[]{:S(2)}) async-start(), calls=%async_computation.9 | async-start | bytes 655360 | tf_op jit(solution)/shard_map/reduce_scatter | solution.py:41
Sparse Core Ops, SparseCore 0:
  563.2 27.5 all-gather.2
  654.0 29.5 reduce-scatter.2
  685.9 21.8 reduce-scatter.4
where the time goes:
time: 718 us; the launch traced here: 716 us
  waiting for transfers between devices  293 us (41%)
  local copies, waits for them, and re-layouts  161 us (22%)
  other arithmetic  112 us (16%)
  blocking collectives  96.3 us (13%)
  starting transfers between devices  22.2 us (3%)
  matrix products  16.6 us (2%)
  between operations  14.5 us (2%)
    all_to_all x1, waiting for transfers between devices, body(): lax.all_to_all(up_tp, 'fs', split_axis=2, concat_axis=1, tiled=True)  148 us
    unnamed x26, local copies, waits for them, and re-layouts  113 us
    unnamed x3, other arithmetic  96.4 us
    all_to_all x1, waiting for transfers between devices, body(): lax.all_to_all(gate_tp, 'fs', split_axis=2, concat_axis=1, tiled=True)  90.4 us
    all_to_all x1, blocking collectives, body(): lax.all_to_all(gate_cast, 'tp', split_axis=0, concat_axis=2, tiled=True)  86.2 us
    reduce_scatter x1, waiting for transfers between devices, body(): by_feature = lax.psum_scatter(term, 'tp', scatter_dimension=1, tiled=True)  29.7 us
  transfers between devices with their start and end apart: 7, of which 6 were waited for; matrix products, arithmetic and copies ran while one was open for 33% of the time, Pallas kernels for 0%

commit v1 on v0

--- a/solution.py
+++ b/solution.py
@@ -9,7 +9,12 @@
     up_cast = (w_up * gain[None, :, None]).astype(jnp.bfloat16)
     down_cast = w_down.astype(jnp.bfloat16)
     gate_tp, up_tp, down_served = (
-        lax.all_to_all(gate_cast, "tp", split_axis=0, concat_axis=2, tiled=True),
+        jnp.concatenate(
+            lax.all_to_all(
+                jnp.stack(jnp.split(gate_cast, lax.axis_size("tp"), axis=0)), "tp", 0, 0
+            ),
+            axis=2,
+        ),
         lax.all_to_all(up_cast, "tp", split_axis=0, concat_axis=2, tiled=True),
         lax.all_to_all(down_cast, "tp", split_axis=0, concat_axis=2, tiled=True),
     )

time: 718 us -> 719 us (level)
    all_to_all x1 -> x0, local copies, waits for them, and re-layouts: 13.7 us -> none  [body(): lax.all_to_all(gate_cast, 'tp', split_axis=0, concat_axis=2, tiled=True)]
    reshape x0 -> x1, local copies, waits for them, and re-layouts: none -> 13.7 us  [body(): jnp.concatenate(lax.all_to_all(jnp.stack(jnp.split(gate_cast, lax.axis_si...]
where the time goes in v1:
time: 719 us; the launch traced here: 717 us
  waiting for transfers between devices  293 us (41%)
  local copies, waits for them, and re-layouts  161 us (22%)
  other arithmetic  113 us (16%)
  blocking collectives  96.3 us (13%)
  starting transfers between devices  22.2 us (3%)
  matrix products  16.6 us (2%)
  between operations  14.5 us (2%)
    all_to_all x1, waiting for transfers between devices, body(): lax.all_to_all(up_tp, 'fs', split_axis=2, concat_axis=1, tiled=True)  148 us
    unnamed x26, local copies, waits for them, and re-layouts  113 us
    unnamed x3, other arithmetic  96.4 us
    all_to_all x1, waiting for transfers between devices, body(): lax.all_to_all(gate_tp, 'fs', split_axis=2, concat_axis=1, tiled=True)  90.4 us
    all_to_all x1, blocking collectives, body(): lax.all_to_all(jnp.stack(jnp.split(gate_cast, lax.axis_size('tp'), axis=0...  86.2 us
    reduce_scatter x1, waiting for transfers between devices, body(): by_feature = lax.psum_scatter(term, 'tp', scatter_dimension=1, tiled=True)  29.7 us
  transfers between devices with their start and end apart: 7, of which 6 were waited for; matrix products, arithmetic and copies ran while one was open for 33% of the time, Pallas kernels for 0%

profile of v1, /device:TPU:0, one launch (start us, length us, event | category | flops | bytes accessed | tf_op | source)
XLA Modules:
  0.0 717.4 jit_solution(3461163147603590616)
XLA Ops:
  7.2 14.3 %copy.30 = f32[4,512,1792]{1,2,0:T(8,128)} copy(f32[4,512,1792]{2,1,0:T(8,128)} %param.11) | data formatting | bytes 29360128 | tf_op args[4]
  21.5 14.3 %copy.34 = f32[4,512,1792]{1,2,0:T(8,128)} copy(f32[4,512,1792]{2,1,0:T(8,128)} %param.12) | data formatting | bytes 29360128 | tf_op args[5]
  35.8 13.5 %multiply_convert_fusion = (bf16[4,512,1792]{1,2,0:T(8,128)(2,1)}, bf16[4,512,1792]{1,2,0:T(8,128)(2,1)S(1)}) fusion(f32[4,512,1792]{1,2,0:T(8,128)} %copy.34, f32[512]{0:T(512)S(1)} %copy-done.1, f32[4,512,1792]{1,2,0:T(8,128)} %copy.30), kind=kLoop, calls=%fused_computation | loop fusion | flops 14680064 | bytes 44042240 | tf_op jit(solution)/shard_map/convert_element_type | solution.py:9
  49.8 1.0 pad_maximum_fusion
  50.8 86.2 %all_to_all.77 = bf16[4,1,512,1792]{2,3,1,0:T(8,128)(2,1)} all-to-all(bf16[4,1,512,1792]{2,3,1,0:T(8,128)(2,1)S(1)} %pad_maximum_fusion), channel_id=1, replica_groups=mesh['grp'=2,'fs'=4,'tp'=4] {'tp'}, dimensions={0} | all-to-all | bytes 14680064 | tf_op jit(solution)/shard_map/all_to_all | solution.py:13
  137.0 5.4 all-to-all-start.2
  142.4 13.7 %copy.46 = bf16[1,512,7168]{1,0,2:T(2,128)(2,1)} copy(bf16[1,512,7168]{1,2,0:T(8,128)(2,1)} %bitcast.55) | data formatting | bytes 14680064 | tf_op jit(solution)/shard_map/reshape | solution.py:12
  156.6 48.2 %reduce = bf16[7168,512]{1,0:T(8,128)(2,1)} reduce(bf16[7168,1,512]{2,1,0:T(2,128)(2,1)} %bitcast.51, bf16[]{:T(256)} %broadcast.43), dimensions={1}, to_apply=%bitcast.50.reduce_sub_computation | reduce | bytes 14680066
  204.9 9.0 %reshape.63 = bf16[4,2,458752]{2,1,0:T(2,128)(2,1)} reshape(bf16[7168,512]{1,0:T(8,128)(2,1)} %reduce) | data formatting | bytes 14680064
  213.8 10.5 %all-to-all-done.2 = bf16[4,512,1792]{1,2,0:T(8,128)(2,1)} async-done(((bf16[4,512,1792]{1,2,0:T(8,128)(2,1)}), bf16[4,512,1792]{1,2,0:T(8,128)(2,1)}, u32[]{:S(2)}, u32[]{:S(2)}) %all-to-all-start.2) | async-done | bytes 7340064 | tf_op jit(solution)/shard_map/all_to_all | solution.py:18
  224.3 5.7 all-to-all-start.1
  230.0 13.7 %copy.45 = bf16[1,512,7168]{1,0,2:T(2,128)(2,1)} copy(bf16[1,512,7168]{1,2,0:T(8,128)(2,1)} %bitcast.11) | data formatting | bytes 14680064 | tf_op jit(solution)/shard_map/all_to_all | solution.py:18
  243.7 48.2 %reduce.1 = bf16[7168,512]{1,0:T(8,128)(2,1)} reduce(bf16[7168,1,512]{2,1,0:T(2,128)(2,1)} %bitcast.52, bf16[]{:T(256)} %broadcast.43), dimensions={1}, to_apply=%bitcast.49.reduce_sub_computation | reduce | bytes 14680066
  291.9 9.0 %reshape.65 = bf16[4,2,458752]{2,1,0:T(2,128)(2,1)} reshape(bf16[7168,512]{1,0:T(8,128)(2,1)} %reduce.1) | data formatting | bytes 14680064
  300.9 90.4 %all-to-all-done.1 = bf16[4,2,458752]{2,1,0:T(2,128)(2,1)} async-done(((bf16[4,2,458752]{2,1,0:T(2,128)(2,1)}), bf16[4,2,458752]{2,1,0:T(2,128)(2,1)}, u32[]{:S(2)}, u32[]{:S(2)}) %all-to-all-start.1) | async-done | bytes 7340064 | tf_op jit(solution)/shard_map/all_to_all | solution.py:22
  391.3 5.5 all-to-all-start.3
  396.8 11.6 %copy.37 = bf16[4,1792,512]{1,2,0:T(8,128)(2,1)} copy(f32[4,1792,512]{2,1,0:T(8,128)} %param.13) | data formatting | bytes 22020096 | tf_op args[6]
  408.5 148.5 %all-to-all-done.3 = bf16[4,2,458752]{2,1,0:T(2,128)(2,1)} async-done(((bf16[4,2,458752]{2,1,0:T(2,128)(2,1)}), bf16[4,2,458752]{2,1,0:T(2,128)(2,1)}, u32[]{:S(2)}, u32[]{:S(2)}) %all-to-all-start.3) | async-done | bytes 7340064 | tf_op jit(solution)/shard_map/all_to_all | solution.py:23
  556.9 5.4 all-to-all-start.4
  565.0 10.1 %all-reduce = bf16[256]{0:T(256)(128)(2,1)S(1)} all-reduce(bf16[256]{0:T(256)(128)(2,1)S(1)} %dynamic-update-slice), channel_id=2, replica_groups=mesh['grp'=2,'fs'=4,'tp'=4] {'fs'}, use_global_device_ids=true, to_apply=%add | all-reduce | flops 256 | bytes 1024
  575.2 11.3 %reshape.64 = bf16[7168,1,512]{2,1,0:T(2,128)(2,1)} reshape(bf16[4,2,458752]{2,1,0:T(2,128)(2,1)} %all-to-all-done.1) | data formatting | bytes 14680064
  586.5 10.4 %copy.41 = bf16[1,512,7168]{1,2,0:T(8,128)(2,1)} copy(bf16[1,512,7168]{1,0,2:T(2,128)(2,1)} %bitcast.53) | data formatting | bytes 14680064
  596.9 9.9 %copy.33 = bf16[1,4,512,1792]{3,2,1,0:T(8,128)(2,1)} copy(bf16[1,4,512,1792]{2,3,1,0:T(8,128)(2,1)} %bitcast.56) | data formatting | bytes 14680064 | tf_op jit(solution)/shard_map/all_to_all | solution.py:22
  606.8 11.3 %reshape.66 = bf16[7168,1,512]{2,1,0:T(2,128)(2,1)} reshape(bf16[4,2,458752]{2,1,0:T(2,128)(2,1)} %all-to-all-done.3) | data formatting | bytes 14680064
  618.1 10.4 %copy.42 = bf16[1,512,7168]{1,2,0:T(8,128)(2,1)} copy(bf16[1,512,7168]{1,0,2:T(2,128)(2,1)} %bitcast.54) | data formatting | bytes 14680064
  628.5 9.9 %copy.36 = bf16[1,4,512,1792]{3,2,1,0:T(8,128)(2,1)} copy(bf16[1,4,512,1792]{2,3,1,0:T(8,128)(2,1)} %bitcast.57) | data formatting | bytes 14680064 | tf_op jit(solution)/shard_map/all_to_all | solution.py:23
  638.5 5.5 fusion.7
  644.3 11.1 %fusion.2 = f32[256,2048]{1,0:T(8,128)} fusion(bf16[1792,2048]{0,1:T(8,128)(2,1)} %bitcast.22, bf16[256,2048]{1,0:T(8,128)(2,1)S(1)} %copy-done.4, bf16[2048,1792]{1,0:T(8,128)(2,1)} %bitcast.60, f32[256,1792]{1,0:T(8,128)S(1)} %fusion.7, f32[256]{0:T(256)S(1)} %convert_element_type.41), kind=kOutput, calls=%fused_computation.10 | convolution fusion | flops 3761307648 | bytes 19661824 | tf_op jit(solution)/shard_map/dot_general | solution.py:44
  655.5 29.7 %reduce-scatter.3.cloned.1.call-done = f32[256,512]{1,0:T(8,128)} async-done(((f32[256,2048]{1,0:T(8,128)}), f32[256,512]{1,0:T(8,128)}) %reduce-scatter.3.cloned.1.call-update) | async-done | bytes 524304 | tf_op jit(solution)/shard_map/reduce_scatter | solution.py:45
  685.2 10.4 %copy.40 = bf16[1,1792,2048]{2,1,0:T(8,128)(2,1)} copy(bf16[1,1792,2048]{1,2,0:T(8,128)(2,1)} %bitcast.16) | data formatting | bytes 14680064
  695.6 13.7 %reduce-scatter.5.cloned.1.call-done = f32[64,512]{1,0:T(8,128)} async-done(((f32[256,512]{1,0:T(8,128)}), f32[64,512]{1,0:T(8,128)}) %reduce-scatter.5.cloned.1.call-update) | async-done | bytes 131088 | tf_op jit(solution)/shard_map/reduce_scatter | solution.py:46
  709.3 1.5 convert_element_type.38
  (30 shorter events, 3.3 us)
Async XLA Ops:
  21.5 14.3 %copy-start.1 = (f32[512]{0:T(512)S(1)}, f32[512]{0:T(512)}, u32[]{:S(2)}) copy-start(f32[512]{0:T(512)} %param.10) | copy-start | bytes 6148
  137.0 87.3 %all-to-all-start.2 = ((bf16[4,512,1792]{1,2,0:T(8,128)(2,1)}), bf16[4,512,1792]{1,2,0:T(8,128)(2,1)}, u32[]{:S(2)}, u32[]{:S(2)}) async-start(bf16[4,512,1792]{1,2,0:T(8,128)(2,1)} %get-tuple-element.20), calls=%async_computation.2 | async-start | bytes 14680064 | tf_op jit(solution)/shard_map/all_to_all | solution.py:18
  224.3 167.0 %all-to-all-start.1 = ((bf16[4,2,458752]{2,1,0:T(2,128)(2,1)}), bf16[4,2,458752]{2,1,0:T(2,128)(2,1)}, u32[]{:S(2)}, u32[]{:S(2)}) async-start(bf16[4,2,458752]{2,1,0:T(2,128)(2,1)} %reshape.63), calls=%async_computation.1 | async-start | bytes 14680064 | tf_op jit(solution)/shard_map/all_to_all | solution.py:22
  391.3 165.6 %all-to-all-start.3 = ((bf16[4,2,458752]{2,1,0:T(2,128)(2,1)}), bf16[4,2,458752]{2,1,0:T(2,128)(2,1)}, u32[]{:S(2)}, u32[]{:S(2)}) async-start(bf16[4,2,458752]{2,1,0:T(2,128)(2,1)} %reshape.65), calls=%async_computation.3 | async-start | bytes 14680064 | tf_op jit(solution)/shard_map/all_to_all | solution.py:23
  408.5 154.0 %copy-start = (bf16[64,2048]{1,0:T(8,128)(2,1)S(1)}, bf16[64,2048]{1,0:T(8,128)(2,1)}, u32[]{:S(2)}) copy-start(bf16[64,2048]{1,0:T(8,128)(2,1)} %param.7) | copy-start | bytes 786436
  408.5 155.0 %copy-start.5 = (u32[32]{0:T(128)S(1)}, u32[32]{0:T(128)}, u32[]{:S(2)}) copy-start(u32[32]{0:T(128)} %constant.19) | copy-start | bytes 388
  408.5 156.3 %copy-start.2 = (s32[64,2]{0,1:T(2,128)S(1)}, s32[64,2]{0,1:T(2,128)}, u32[]{:S(2)}) copy-start(s32[64,2]{0,1:T(2,128)} %param.8) | copy-start | bytes 1540
  408.5 156.3 %copy-start.3 = (f32[64,2]{0,1:T(2,128)S(1)}, f32[64,2]{0,1:T(2,128)}, u32[]{:S(2)}) copy-start(f32[64,2]{0,1:T(2,128)} %param.9) | copy-start | bytes 1540
  556.9 87.3 %all-to-all-start.4 = ((bf16[4,1792,512]{1,2,0:T(8,128)(2,1)}), bf16[4,1792,512]{1,2,0:T(8,128)(2,1)}, u32[]{:S(2)}, u32[]{:S(2)}) async-start(bf16[4,1792,512]{1,2,0:T(8,128)(2,1)} %copy.37), calls=%async_computation.4 | async-start | bytes 14680064 | tf_op jit(solution)/shard_map/all_to_all | solution.py:19
  562.4 76.1 %all-gather.3.cloned.1.call-start = ((), (), s32[]{:S(2)}) async-start(), calls=%async_computation.7 | async-start | bytes 1310720 | tf_op jit(solution)/shard_map/all_gather | solution.py:37
  563.4 121.7 %reduce-scatter.3.cloned.1.call-start = ((), (), s32[]{:S(2)}) async-start(), calls=%async_computation.8 | async-start | bytes 2621440 | tf_op jit(solution)/shard_map/reduce_scatter | solution.py:45
  638.5 5.8 copy-start.4
  655.4 53.9 %reduce-scatter.5.cloned.1.call-start = ((), (), s32[]{:S(2)}) async-start(), calls=%async_computation.9 | async-start | bytes 655360 | tf_op jit(solution)/shard_map/reduce_scatter | solution.py:46
Sparse Core Ops, SparseCore 0:
  564.7 27.5 all-gather.2
  655.5 29.5 reduce-scatter.2
  687.4 21.8 reduce-scatter.4
